TPU v7x, 256 devices: a whole 4x4x8 slice. The times are simulated.
256 devices in a mesh: sp: 128 (over z, y, x), tp: 2 (over core).
Axes of the slice: x: 4, y: 4, z: 8, core: 2. Of those that a mesh axis runs over, the one named last changes fastest.
Arguments:
- tokens: bfloat16 [49152, 2048], P('sp', 'tp'), may hold values from -1620 to 1620
- input_norm_gain: float32 [2048], replicated, may hold values from 0.1 to 1.9
- outer_gate_weight: bfloat16 [2048, 1024], P(None, 'tp'), may hold values from -0.125 to 0.125
- inner_gate_weight: bfloat16 [2048, 1024], P(None, 'tp'), may hold values from -0.125 to 0.125
- convolution_input_weight: bfloat16 [2048, 1024], P(None, 'tp'), may hold values from -0.125 to 0.125
- convolution_kernel_taps: bfloat16 [3, 1024], P(None, 'tp'), may hold values from -3 to 3
- query_weight_matrix: bfloat16 [2048, 512], P(None, 'tp'), may hold values from -0.125 to 0.125
- key_weight_matrix: bfloat16 [2048, 512], P(None, 'tp'), may hold values from -0.125 to 0.125
- value_weight_matrix: bfloat16 [2048, 1024], P(None, 'tp'), may hold values from -0.125 to 0.125
- forget_gate_weight: bfloat16 [2048, 512], P(None, 'tp'), may hold values from -0.125 to 0.125
- attention_gate_weight: bfloat16 [2048, 1024], P(None, 'tp'), may hold values from -0.125 to 0.125
- forget_gate_bias: float32 [512], P('tp'), may hold values from -1.5 to 10
- extra_logarithm_decay: float32 [49152, 16], P('sp', 'tp'), may hold values from -0.72 to 0
- initial_head_state: float32 [16, 32, 64], P('tp'), may hold values from -768 to 768
- head_norm_gain: float32 [64], replicated, may hold values from 0.1 to 1.9
- convolution_output_weight: bfloat16 [1024, 2048], P('tp'), may hold values from -0.125 to 0.125
- attention_output_weight: bfloat16 [1024, 2048], P('tp'), may hold values from -0.125 to 0.125
Outputs:
- mixed: bfloat16 [49152, 2048], P(('sp', 'tp'))
All inputs are finite; a program needn't handle non-finite values.
Results may differ from a plain program's by a relative error of at most 0.017.
Values may be sent and summed in bfloat16 or wider, within the bound.
A program may use at most 128 MiB of HBM per device.

v0:
```python
import jax
import jax.numpy as jnp
from jax import lax
from jax.sharding import Mesh
from jax.sharding import PartitionSpec as P

BLOCK = 64
SP = ("sp_0", "sp_1", "sp_2")
SP_TP = ("sp_0", "sp_1", "sp_2", "tp")


NORM_EPS = 1e-06
GATE_SOFTNESS = 16.0


def joined_along(parts, dim):
    parts = jnp.moveaxis(parts, 0, dim)
    lengths = parts.shape
    return parts.reshape(*lengths[:dim], lengths[dim] * lengths[dim + 1], *lengths[dim + 2 :])


def sent_to_all(shard, axis):
    length = lax.axis_size(axis)
    return lax.all_to_all(
        jnp.broadcast_to(shard[None], (length, *shard.shape)), axis, 0, 0, tiled=True
    )


def gather_directly(shard, axis, dim):
    return joined_along(sent_to_all(shard, axis), dim)


def from_behind(block, axis, distance):
    devices = range(lax.axis_size(axis))
    route = [(i - distance, i) for i in devices if i - distance in devices]
    return lax.ppermute(block, axis, route)


def filled_with(shard, identity):
    return jax.tree.map(
        lambda a, e: jnp.broadcast_to(jnp.asarray(e, a.dtype), a.shape), shard, identity
    )


def collected_together(shard, axis):
    leaves = jax.tree.leaves(shard)
    order = sorted(range(len(leaves)), key=lambda k: -leaves[k].size)
    width = (1, *leaves[order[0]].shape)[-1]
    lines = [
        jnp.pad(leaves[k].reshape(-1), (0, -leaves[k].size % width)).reshape(-1, width)
        for k in order
    ]
    both, at, found = (lax.all_gather(jnp.concatenate(lines), axis), 0, {})
    for k, line in zip(order, lines):
        piece = both[:, at : at + len(line)].reshape(len(both), -1)
        found[k] = piece[:, : leaves[k].size].reshape(-1, *leaves[k].shape)
        at += len(line)
    numbers = iter(range(len(leaves)))
    return jax.tree.map(lambda _: found[next(numbers)], shard)


def entering_2(shard, axes, combine, identity):
    before = start = filled_with(shard, identity)
    so_far = shard
    for axis in reversed(axes):
        length, here = (lax.axis_size(axis), lax.axis_index(axis))
        pieces = collected_together(so_far, axis)
        inside, so_far = (start, start)
        for k in range(length):
            passed = k < here
            so_far = combine(so_far, jax.tree.map(lambda part: part[k], pieces))
            inside = jax.tree.map(lambda new, old: jnp.where(passed, new, old), so_far, inside)
        before = combine(inside, before)
    return before


def split_up(shard, dim, length):
    lengths = shard.shape
    parts = shard.reshape(*lengths[:dim], length, lengths[dim] // length, *lengths[dim + 1 :])
    return jnp.moveaxis(parts, dim, 0)


def sent_and_summed(shard, axis, dim):
    parts = split_up(shard, dim, lax.axis_size(axis))
    arrived = lax.all_to_all(parts, axis, split_axis=0, concat_axis=0, tiled=True)
    return arrived.astype(jnp.float32).sum(axis=0)


def block_terms(queries, key_rows, values, logarithm_decay):
    cumulative = jnp.cumsum(logarithm_decay, axis=1)
    last_log = cumulative[:, -1:]
    query_g = queries * jnp.exp(cumulative)
    key_g = key_rows * jnp.exp(-cumulative)
    scores = jnp.einsum("nihd,njhd->nhij", query_g, key_g, precision=lax.Precision.HIGHEST)
    width = queries.shape[1]
    causal = jnp.arange(width)[:, None] >= jnp.arange(width)[None, :]
    scores = jnp.where(causal, scores, 0.0)
    inner = jnp.einsum("nhij,njhe->nihe", scores, values, precision=lax.Precision.HIGHEST)
    key_decayed = key_rows * jnp.exp(last_log - cumulative)
    update = jnp.einsum("nchd,nche->nhde", key_decayed, values, precision=lax.Precision.HIGHEST)
    return (query_g, inner, update, last_log[:, 0])


def carry_step(state, inputs):
    block_decay, update = inputs
    return (block_decay[..., None] * state + update, state)


def chain_join(earlier, later):
    return (earlier[0] * later[0], later[0][..., None] * earlier[1] + later[1])


def on_device(
    tokens,
    input_norm_gain,
    outer_gate_weight,
    inner_gate_weight,
    convolution_input_weight,
    convolution_kernel_taps,
    query_weight_matrix,
    key_weight_matrix,
    value_weight_matrix,
    forget_gate_weight,
    attention_gate_weight,
    forget_gate_bias,
    extra_logarithm_decay,
    initial_head_state,
    head_norm_gain,
    convolution_output_weight,
    attention_output_weight,
):
    number_of_rows = tokens.shape[0]
    number_of_heads, key_channel_count, value_dim = initial_head_state.shape
    weights = (
        outer_gate_weight,
        inner_gate_weight,
        convolution_input_weight,
        query_weight_matrix,
        key_weight_matrix,
        value_weight_matrix,
        forget_gate_weight,
        attention_gate_weight,
    )
    whole_rows = gather_directly(tokens, "tp", 1).astype(jnp.float32)
    power = jnp.mean(whole_rows * whole_rows, axis=1, keepdims=True)
    normed = (whole_rows * lax.rsqrt(power + NORM_EPS) * input_norm_gain).astype(jnp.bfloat16)
    sums = tuple(
        (jnp.dot(normed, weight, preferred_element_type=jnp.float32) for weight in weights)
    )
    conv_b, conv_c, conv_h, query, key_proj, value, forget_preactivation, out_gate = (
        term.astype(jnp.bfloat16) for term in sums
    )
    product = (conv_c.astype(jnp.float32) * conv_h.astype(jnp.float32)).astype(jnp.bfloat16)
    tap_count = convolution_kernel_taps.shape[0]
    previous = from_behind(product[number_of_rows - tap_count + 1 :], SP, 1)
    padded = jnp.concatenate([previous, product], axis=0)
    conv = jnp.zeros(product.shape, jnp.float32)
    for tap_index in range(tap_count):
        conv = conv + convolution_kernel_taps[tap_index].astype(jnp.float32) * padded[
            tap_index : tap_index + number_of_rows
        ].astype(jnp.float32)
    conv_out = (conv_b.astype(jnp.float32) * conv).astype(jnp.bfloat16)
    logarithm_decay = (
        jax.nn.log_sigmoid(forget_preactivation.astype(jnp.float32) + forget_gate_bias)
        / GATE_SOFTNESS
    )
    logarithm_decay = (
        logarithm_decay.reshape(number_of_rows, number_of_heads, key_channel_count)
        + extra_logarithm_decay[:, :, None]
    )
    n_blocks = number_of_rows // BLOCK
    queries = (query.astype(jnp.float32) * key_channel_count ** (-0.5)).reshape(
        n_blocks, BLOCK, number_of_heads, key_channel_count
    )
    key_rows = key_proj.astype(jnp.float32).reshape(
        n_blocks, BLOCK, number_of_heads, key_channel_count
    )
    values = value.astype(jnp.float32).reshape(n_blocks, BLOCK, number_of_heads, value_dim)
    query_g, inner, update, block_log = block_terms(
        queries,
        key_rows,
        values,
        logarithm_decay.reshape(n_blocks, BLOCK, number_of_heads, key_channel_count),
    )
    zero_state = jnp.zeros((number_of_heads, key_channel_count, value_dim), jnp.float32)
    local_final, entering = lax.scan(carry_step, zero_state, (jnp.exp(block_log), update))
    exclusive = jnp.cumsum(block_log, axis=0) - block_log
    device_decay = jnp.exp(jnp.sum(block_log, axis=0))
    prefix_decay, prefix_state = entering_2(
        (device_decay, local_final), SP, chain_join, (jnp.ones_like(device_decay), zero_state)
    )
    incoming = prefix_state + prefix_decay[..., None] * initial_head_state
    entering = entering + jnp.exp(exclusive)[..., None] * incoming[None]
    outer = jnp.einsum("nchd,nhde->nche", query_g, entering, precision=lax.Precision.HIGHEST)
    raw = (inner + outer).reshape(number_of_rows, number_of_heads, value_dim)
    raw = raw * lax.rsqrt(jnp.mean(raw * raw, axis=2, keepdims=True) + NORM_EPS) * head_norm_gain
    gate_values = jax.nn.silu(out_gate.astype(jnp.float32)).reshape(
        number_of_rows, number_of_heads, value_dim
    )
    attn_out = (
        (raw * gate_values)
        .reshape(number_of_rows, number_of_heads * value_dim)
        .astype(jnp.bfloat16)
    )
    mixed = sent_and_summed(
        (
            jnp.dot(conv_out, convolution_output_weight, preferred_element_type=jnp.float32)
            + jnp.dot(attn_out, attention_output_weight, preferred_element_type=jnp.float32)
        ).astype(jnp.bfloat16),
        "tp",
        0,
    )
    return mixed.astype(jnp.bfloat16)


def solution(mesh):
    torus = Mesh(mesh.devices.reshape(8, 4, 4, mesh.shape["tp"]), ("sp_0", "sp_1", "sp_2", "tp"))
    return jax.shard_map(
        on_device,
        mesh=torus,
        in_specs=(
            P(SP, "tp"),
            P(),
            P(None, "tp"),
            P(None, "tp"),
            P(None, "tp"),
            P(None, "tp"),
            P(None, "tp"),
            P(None, "tp"),
            P(None, "tp"),
            P(None, "tp"),
            P(None, "tp"),
            P("tp"),
            P(SP, "tp"),
            P("tp", None, None),
            P(),
            P("tp", None),
            P("tp", None),
        ),
        out_specs=P(SP_TP, None),
        check_vma=False,
    )
```

profile of v0, /device:TPU:1, one launch (start us, length us, event | category | flops | bytes accessed | tf_op | source)
XLA Modules:
  0.0 187.9 jit_solution(4163360113792740572)
XLA Ops:
  0.0 1.6 copy.87
  1.8 7.8 %all_to_all.10 = bf16[2,384,1024]{1,2,0:T(8,128)(2,1)S(1)} all-to-all(bf16[2,384,1024]{1,2,0:T(8,128)(2,1)S(1)} %broadcast_in_dim.25), channel_id=1, replica_groups=mesh['sp_0'=8,'sp_1'=4,'sp_2'=4,'tp'=2] {'tp'}, dimensions={0} | all-to-all | bytes 3145728 | tf_op jit(solution)/shard_map/all_to_all | solution.py:24
  16.4 2.0 %collective-permute-start = (bf16[2,512]{1,0:T(2,128)(2,1)}, bf16[2,512]{1,0:T(2,128)(2,1)}, u32[]{:S(2)}, u32[]{:S(2)}) collective-permute-start(bf16[2,512]{1,0:T(2,128)(2,1)} %slice.226), channel_id=1, source_target_pairs={{0,2},{2,4},{4,6},{6,8},{8,10},{10,12},{12,14},{14,16},{16,18},{18... | collective-permute-start | bytes 6152 | tf_op jit(solution)/shard_map/ppermute | solution.py:36
  19.1 2.5 %fusion.41 = f32[384,256]{1,0:T(8,128)S(1)} fusion(bf16[384,2048]{0,1:T(8,128)(2,1)} %copy-done.1, bf16[2048,256]{1,0:T(8,128)(2,1)} %param.28, f32[256]{0:T(256)S(1)} %copy-done.48), kind=kOutput, calls=%fused_computation.65 | convolution fusion | flops 403832832 | bytes 3015680 | tf_op jit(solution)/shard_map/dot_general | solution.py:148
  22.5 1.2 reshape.387
  24.7 2.9 %copy.90 = f32[6,64,8,32]{3,2,1,0:T(8,128)} copy(f32[6,64,8,32]{1,0,3,2:T(8,128)} %broadcast_add_fusion) | data formatting | bytes 786432 | tf_op jit(solution)/shard_map/add | solution.py:168
  27.6 1.5 fusion.66
  30.4 2.4 %fusion.16 = f32[384,256]{1,0:T(8,128)S(1)} fusion(bf16[384,2048]{0,1:T(8,128)(2,1)} %copy-done.1, bf16[2048,256]{1,0:T(8,128)(2,1)} %param.26), kind=kOutput, calls=%fused_computation.34 | convolution fusion | flops 402849792 | bytes 3014656 | tf_op jit(solution)/shard_map/dot_general | solution.py:148
  32.8 2.8 %fusion.21 = f32[384,256]{1,0:T(8,128)} fusion(bf16[384,2048]{0,1:T(8,128)(2,1)S(1)} %copy-done.2, bf16[2048,256]{1,0:T(8,128)(2,1)} %param.25), kind=kOutput, calls=%fused_computation.41 | convolution fusion | flops 402948096 | bytes 3014656 | tf_op jit(solution)/shard_map/dot_general | solution.py:148
  35.6 1.8 convolution_convert_fusion.1
  37.3 1.5 reshape.385
  39.0 2.7 %reshape.411 = f32[6,64,8,32]{3,2,1,0:T(8,128)} reshape(f32[384,256]{1,0:T(8,128)} %fusion.21) | data formatting | bytes 786432 | tf_op jit(solution)/shard_map/reshape | solution.py:172
  41.7 1.6 reshape.412
  43.3 4.7 %exponential_multiply_fusion = (f32[6,64,8,32]{3,2,1,0:T(8,128)S(1)}, f32[6,64,8,32]{3,2,1,0:T(8,128)}, f32[6,64,8,32]{3,2,1,0:T(8,128)}) fusion(f32[6,64,8,32]{3,2,1,0:T(8,128)} %reshape.412, f32[6,64,8,32]{3,2,1,0:T(8,128)} %copy-done.5, f32[6,8,32]{2,1,0:T(8,128)S(1)} %get-tuple-element.69, f32[6,64,8,32]{3,2,1,0:T(8,128)} %reshape.411), kind=kLoop, calls=%fused_computation.14 | loop fusion | flops 491520 | bytes 2365440 | tf_op jit(solution)/shard_map/mul | solution.py:99
  48.0 2.3 %fusion.2 = f32[6,8,32,64]{3,2,1,0:T(8,128)} fusion(f32[6,64,8,32]{3,2,1,0:T(8,128)S(1)} %get-tuple-element.66, bf16[6,64,8,64]{3,2,1,0:T(8,128)(2,1)S(1)} %reshape.385), kind=kOutput, calls=%fused_computation.8 | convolution fusion | flops 75497472 | bytes 1179648 | tf_op jit(solution)/shard_map/nchd,nche->nhde/dot_general | solution.py:100
  50.3 10.3 %while.13 = (s32[]{:T(128)}, f32[8,32,64]{2,1,0:T(8,128)S(1)}, f32[6,8,32,64]{3,2,1,0:T(8,128)}, f32[6,8,32]{2,1,0:T(8,128)S(1)}, f32[6,8,32,64]{3,2,1,0:T(8,128)}, /*index=5*/s32[]{:T(128)}, s32[]{:T(128)}) while((s32[]{:T(128)}, f32[8,32,64]{2,1,0:T(8,128)S(1)}, f32[6,8,32,64]{3,2,1,0:T(8,128)}, f32[6,8,32]{2,1,0:T(8,128)S(1)}, ...), condition=%wide.region_3.4_spmd.clone, body=%wide.region_2.3_spmd.clone.sunk | while | flops 65539 | bytes 396396 | solution.py:186
  60.7 10.3 %all-gather.3 = f32[4,260,64]{1,2,0:T(8,128)S(1)} all-gather(f32[1,260,64]{1,2,0:T(8,128)S(1)} %copy.100), channel_id=2, replica_groups=mesh['sp_0'=8,'sp_1'=4,'sp_2'=4,'tp'=2] {'sp_2'}, dimensions={0}, use_global_device_ids=true | all-gather | bytes 332800 | tf_op jit(solution)/shard_map/all_gather | solution.py:53
  73.3 9.9 %all-gather.4 = f32[4,260,64]{1,2,0:T(8,128)S(1)} all-gather(f32[1,260,64]{1,2,0:T(8,128)S(1)} %copy.109), channel_id=3, replica_groups=mesh['sp_0'=8,'sp_1'=4,'sp_2'=4,'tp'=2] {'sp_1'}, dimensions={0}, use_global_device_ids=true | all-gather | bytes 332800 | tf_op jit(solution)/shard_map/all_gather | solution.py:53
  86.8 23.8 %all-gather.5 = f32[8,260,64]{1,2,0:T(8,128)S(1)} all-gather(f32[1,260,64]{1,2,0:T(8,128)S(1)} %copy.118), channel_id=4, replica_groups=mesh['sp_0'=8,'sp_1'=4,'sp_2'=4,'tp'=2] {'sp_0'}, dimensions={0}, use_global_device_ids=true | all-gather | bytes 599040 | tf_op jit(solution)/shard_map/all_gather | solution.py:53
  124.0 1.6 copy.157
  125.6 1.6 copy.163
  131.7 1.9 copy.94
  134.3 4.4 %fusion.4 = f32[6,8,64,64]{3,2,1,0:T(8,128)S(1)} fusion(f32[6,64,8,32]{1,3,2,0:T(8,128)S(1)} %copy.94, f32[6,64,8,32]{3,2,1,0:T(8,128)} %get-tuple-element.67), kind=kOutput, calls=%fused_computation.10 | convolution fusion | flops 75497472 | bytes 1572864 | tf_op jit(solution)/shard_map/nihd,njhd->nhij/dot_general | solution.py:94
  138.9 1.5 fusion.6
  141.7 4.1 %multiply_reduce_fusion.1 = (f32[6,64,8]{1,2,0:T(8,128)S(1)}, f32[6,64,8,64]{1,3,2,0:T(8,128)}) fusion(f32[6,8,64,64]{3,2,1,0:T(8,128)S(1)} %fusion.6, f32[6,64,8,32]{1,3,2,0:T(8,128)S(1)} %copy.94, f32[6,8,32,64]{3,2,1,0:T(8,128)S(1)} %copy-done.13, f32[8,32,64]{2,1,0:T(8,128)S(1)} %multiply_add_fusion, f32[6,8,32]{2,1,0:T(8,128)S(1)} %copy-done.26), kind=kOutput, calls=%fused_computation.12 | convolution fusion | flops 76280832 | bytes 2443264 | tf_op jit(solution)/shard_map/nchd,nhde->nche/dot_general | solution.py:194
  146.1 1.2 copy.138
  147.3 3.0 %copy.136 = f32[6,64,8,64]{3,2,1,0:T(8,128)} copy(f32[6,64,8,64]{1,3,2,0:T(8,128)} %get-tuple-element.111) | data formatting | bytes 1572864 | tf_op jit(solution)/shard_map/add | solution.py:195
  150.4 2.6 %reshape.391 = f32[384,512]{1,0:T(8,128)} reshape(f32[6,64,8,64]{3,2,1,0:T(8,128)} %copy.136) | data formatting | bytes 1572864 | tf_op jit(solution)/shard_map/reshape | solution.py:195
  153.0 5.8 %fusion.23 = f32[384,2048]{1,0:T(8,128)} fusion(bf16[512,2048]{1,0:T(8,128)(2,1)S(1)} %copy-done, bf16[384,2048]{0,1:T(8,128)(2,1)} %copy-done.1, bf16[2048,512]{1,0:T(8,128)(2,1)} %param.21, bf16[384,512]{1,0:T(8,128)(2,1)S(1)} %copy-done.24, bf16[2,512]{1,0:T(2,128)(2,1)} %collective-permute-done, f32[512]{0:T(512)S(1)} %bitcast.148, ...), kind=kOutput, calls=%fused_computation.44 | convolution fusion | flops 1614151680 | bytes 9314304 | tf_op jit(solution)/shard_map/dot_general | solution.py:207
  158.8 7.0 %add_convert_fusion = bf16[384,2048]{1,0:T(8,128)(2,1)} fusion(f32[384,2048]{1,0:T(8,128)} %fusion.23, bf16[512,2048]{1,0:T(8,128)(2,1)} %param.35, bf16[384,2048]{0,1:T(8,128)(2,1)} %copy-done.1, bf16[2048,512]{1,0:T(8,128)(2,1)} %param.29, f32[384,512]{1,0:T(8,128)} %reshape.391, f32[384,512]{1,0:T(8,128)S(1)} %copy-done.14, f32[512]{0:T(512)S(1)} %mul.657), kind=kOutput, calls=%fused_computation.6 | convolution fusion | flops 1614151680 | bytes 12060672 | tf_op jit(solution)/shard_map/dot_general | solution.py:208
  165.8 19.3 %all_to_all.11 = bf16[2,192,2048]{2,1,0:T(8,128)(2,1)} all-to-all(bf16[2,192,2048]{2,1,0:T(8,128)(2,1)} %bitcast.130), channel_id=1, replica_groups=mesh['sp_0'=8,'sp_1'=4,'sp_2'=4,'tp'=2] {'tp'}, dimensions={0} | all-to-all | bytes 3145728 | tf_op jit(solution)/shard_map/all_to_all | solution.py:85
  185.1 2.8 %reduce_sum.42 = bf16[192,2048]{1,0:T(8,128)(2,1)} reduce(bf16[2,192,2048]{2,1,0:T(8,128)(2,1)} %all_to_all.11, bf16[]{:T(256)} %constant.73.clone.1), dimensions={0}, to_apply=%region_7.8 | reduce | flops 393216 | bytes 2359298 | tf_op jit(solution)/shard_map/reduce_sum | solution.py:86
  (216 shorter events, 46.8 us)
Async XLA Ops:
  0.0 153.0 %copy-start = (bf16[512,2048]{1,0:T(8,128)(2,1)S(1)}, bf16[512,2048]{1,0:T(8,128)(2,1)}, u32[]{:S(2)}) copy-start(bf16[512,2048]{1,0:T(8,128)(2,1)} %param.34) | copy-start | bytes 6291460
  11.9 2.2 %copy-start.6 = (bf16[2048,512]{1,0:T(8,128)(2,1)S(1)}, bf16[2048,512]{1,0:T(8,128)(2,1)}, u32[]{:S(2)}) copy-start(bf16[2048,512]{1,0:T(8,128)(2,1)} %param.23) | copy-start | bytes 6291460
  14.1 4.9 %copy-start.42 = (f32[384,8]{0,1:T(8,128)S(1)}, f32[384,8]{0,1:T(8,128)}, u32[]{:S(2)}) copy-start(f32[384,8]{0,1:T(8,128)} %param.31) | copy-start | bytes 36868
  14.1 5.0 %copy-start.48 = (f32[256]{0:T(256)S(1)}, f32[256]{0:T(256)}, u32[]{:S(2)}) copy-start(f32[256]{0:T(256)} %param.30) | copy-start | bytes 3076
  16.4 136.6 %collective-permute-start = (bf16[2,512]{1,0:T(2,128)(2,1)}, bf16[2,512]{1,0:T(2,128)(2,1)}, u32[]{:S(2)}, u32[]{:S(2)}) collective-permute-start(bf16[2,512]{1,0:T(2,128)(2,1)} %slice.226), channel_id=1, source_target_pairs={{0,2},{2,4},{4,6},{6,8},{8,10},{10,12},{12,14},{14,16},{16,18},{18... | collective-permute-start | bytes 6152 | tf_op jit(solution)/shard_map/ppermute | solution.py:36
  30.4 2.4 %copy-start.2 = (bf16[384,2048]{0,1:T(8,128)(2,1)S(1)}, bf16[384,2048]{0,1:T(8,128)(2,1)}, u32[]{:S(2)}) copy-start(bf16[384,2048]{0,1:T(8,128)(2,1)} %copy-done.1) | copy-start | bytes 4718596
  32.8 2.8 %copy-start.47 = (bf16[2048,512]{1,0:T(8,128)(2,1)S(1)}, bf16[2048,512]{1,0:T(8,128)(2,1)}, u32[]{:S(2)}) copy-start(bf16[2048,512]{1,0:T(8,128)(2,1)} %param.27) | copy-start | bytes 6291460
  38.9 9.1 %copy-start.3 = (bf16[6,64,8,64]{3,2,1,0:T(8,128)(2,1)}, bf16[6,64,8,64]{3,2,1,0:T(8,128)(2,1)S(1)}, u32[]{:S(2)}) copy-start(bf16[6,64,8,64]{3,2,1,0:T(8,128)(2,1)S(1)} %reshape.385) | copy-start | bytes 1179652
  86.2 25.8 %copy-start.7 = (f32[1,256,64]{2,1,0:T(8,128)}, f32[1,256,64]{2,1,0:T(8,128)S(1)}, u32[]{:S(2)}) copy-start(f32[1,256,64]{2,1,0:T(8,128)S(1)} %copy.155) | copy-start | bytes 196612
  86.3 25.7 %copy-start.9 = (f32[1,256,64]{2,1,0:T(8,128)}, f32[1,256,64]{2,1,0:T(8,128)S(1)}, u32[]{:S(2)}) copy-start(f32[1,256,64]{2,1,0:T(8,128)S(1)} %copy.154) | copy-start | bytes 196612
  86.4 25.6 %copy-start.11 = (f32[1,256,64]{2,1,0:T(8,128)}, f32[1,256,64]{2,1,0:T(8,128)S(1)}, u32[]{:S(2)}) copy-start(f32[1,256,64]{2,1,0:T(8,128)S(1)} %copy.156) | copy-start | bytes 196612
  114.4 17.3 %copy-start.36 = (f32[8,32]{1,0:T(8,128)}, f32[8,32]{1,0:T(8,128)S(1)}, u32[]{:S(2)}) copy-start(f32[8,32]{1,0:T(8,128)S(1)} %mul.611) | copy-start | bytes 3076
  134.3 4.4 %copy-start.4 = (bf16[6,64,8,64]{3,2,1,0:T(8,128)(2,1)S(1)}, bf16[6,64,8,64]{3,2,1,0:T(8,128)(2,1)}, u32[]{:S(2)}) copy-start(bf16[6,64,8,64]{3,2,1,0:T(8,128)(2,1)} %copy-done.3) | copy-start | bytes 1179652
  134.3 4.4 %copy-start.40 = (pred[64,64]{1,0:T(8,128)(4,1)S(1)}, pred[64,64]{1,0:T(8,128)(4,1)}, u32[]{:S(2)}) copy-start(pred[64,64]{1,0:T(8,128)(4,1)} %iota_compare_fusion) | copy-start | bytes 12292
  138.7 1.8 copy-start.27
  138.8 1.8 copy-start.8
  138.8 1.8 copy-start.10
  138.8 1.8 copy-start.12
  138.8 1.8 copy-start.15
  138.8 1.8 copy-start.16
  138.8 1.8 copy-start.17
  138.8 1.8 copy-start.18
  138.8 1.8 copy-start.19
  138.9 1.8 copy-start.20
  138.9 1.8 copy-start.21
  138.9 1.8 copy-start.22
  138.9 1.8 copy-start.25
  138.9 1.8 copy-start.41
  141.7 4.1 %copy-start.43 = (bf16[3,512]{1,0:T(4,128)(2,1)S(1)}, bf16[3,512]{1,0:T(4,128)(2,1)}, u32[]{:S(2)}) copy-start(bf16[3,512]{1,0:T(4,128)(2,1)} %param.24) | copy-start | bytes 9220
  141.7 4.2 %copy-start.45 = (f32[64]{0:T(128)S(1)}, f32[64]{0:T(128)}, u32[]{:S(2)}) copy-start(f32[64]{0:T(128)} %param.33) | copy-start | bytes 772
  150.4 2.6 %copy-start.24 = (bf16[384,512]{1,0:T(8,128)(2,1)S(1)}, bf16[384,512]{1,0:T(8,128)(2,1)}, u32[]{:S(2)}) copy-start(bf16[384,512]{1,0:T(8,128)(2,1)} %copy-done.23) | copy-start | bytes 1179652
  153.0 5.8 %copy-start.14 = (f32[384,512]{1,0:T(8,128)S(1)}, f32[384,512]{1,0:T(8,128)}, u32[]{:S(2)}) copy-start(f32[384,512]{1,0:T(8,128)} %copy.138) | copy-start | bytes 2359300
  (18 other events, 27.1 us)
where the time goes:
time: 189 us; the launch traced here: 188 us
  blocking collectives  71.1 us (38%)
  local copies, waits for them, and re-layouts  52.3 us (28%)
  matrix products  36.5 us (19%)
  other arithmetic  25.1 us (13%)
  starting transfers between devices  1.97 us (1%)
    all_gather x3, blocking collectives, collected_together(): both, at, found = (lax.all_gather(jnp.concatenate(lines), axis), 0, {})  44 us
    all_to_all x1, blocking collectives, sent_and_summed(): lax.all_to_all(parts, axis, split_axis=0, concat_axis=0, tiled=True)  19.3 us
    unnamed x126, local copies, waits for them, and re-layouts  14.9 us
    dot_general x6, matrix products, on_device(): jnp.dot(normed, weight, preferred_element_type=jnp.float32)  11.4 us
    slice x14, local copies, waits for them, and re-layouts, entering_2(): so_far = combine(so_far, jax.tree.map(lambda part: part[k], pieces))  8.09 us
    all_to_all x1, blocking collectives, sent_to_all(): lax.all_to_all(jnp.broadcast_to(shard[None], (length, *shard.shape)), axi...  7.82 us
    dot_general x1, matrix products, on_device(): jnp.dot(attn_out, attention_output_weight, preferred_element_type=jnp.flo...  7.02 us
    add x6, other arithmetic, carry_step(): return (block_decay[..., None] * state + update, state)  6.13 us
  transfers between devices with their start and end apart: 1, of which 0 were waited for; matrix products, arithmetic and copies ran while one was open for 47% of the time, Pallas kernels for 0%

commit v1 on v0

v1 whole, which is shorter than its diff:
```python
import jax
import jax.numpy as jnp
from jax import lax
from jax.experimental import pallas as pl
from jax.experimental.pallas import tpu as pltpu
from jax.sharding import PartitionSpec as P

F32 = jnp.float32
BF16 = jnp.bfloat16
NORM_EPS = 1e-06
MESH = pl.DeviceIdType.MESH

ROWS = 384
HALF = 1024
BLK = 128
NBLK = ROWS // BLK
PLANE = 16
PLANES = 8
K0, F0, V0, C0, H0, B0, G0, Q0 = 0, 256, 512, 1024, 1536, 2048, 2560, 3072
WIDE = 3328


def split2(x):
    hi = x.astype(BF16)
    lo = (x - hi.astype(F32)).astype(BF16)
    return hi, lo


def split3(x):
    hi = x.astype(BF16)
    rest = x - hi.astype(F32)
    mid = rest.astype(BF16)
    lo = (rest - mid.astype(F32)).astype(BF16)
    return hi, mid, lo


def iota(shape, dim):
    return lax.broadcasted_iota(jnp.int32, shape, dim)


def dot(a, b):
    return jnp.dot(a, b, preferred_element_type=F32)


def dot_t(a, b):
    return lax.dot_general(a, b, (((1,), (1,)), ((), ())), preferred_element_type=F32)


def kernel(
    tok, gain, wb, wc, wh, taps, wq, wk, wv, wf, wg, bias, extra, init, hgain, wco, wao,
    out,
    X, XG, W, WO, PJ, SS, RS, GN, BI, EX, TP_, HG, ST, CUM, KG, QG, QI, QF, EN,
    P1S, P1R, EU, ED, ZS, ZR, P3S, SIN, SBD, INI, PR, CO, RAW, AO, OUT, SB, RB, OB,
    lsem, osem, tok_s, tok_r, p1_s, p1_r, z_s, z_r, p3_s, p3_r, cv_s, cv_r, ot_s, ot_r,
):
    sp = lax.axis_index("sp")
    tp = lax.axis_index("tp")
    other = 1 - tp
    z = sp // PLANE
    p = sp % PLANE
    base = sp - p
    nsp = PLANE * PLANES

    bar = pltpu.get_barrier_semaphore()

    def greet(dev):
        pl.semaphore_signal(bar, inc=1, device_id=dev, device_id_type=MESH)

    greet((sp, other))
    for o in range(1, PLANE):
        greet((base + (p + o) % PLANE, tp))
    for o in range(1, PLANES):
        greet(((z + o) % PLANES * PLANE + p, tp))
    greet(((sp + 1) % nsp, tp))
    greet(((sp + nsp - 1) % nsp, tp))

    n_local = [0]

    def fetch(src, dst):
        c = pltpu.make_async_copy(src, dst, lsem.at[n_local[0]])
        n_local[0] += 1
        c.start()
        return c

    own = pl.ds(pl.multiple_of(tp * HALF, HALF), HALF)
    oth = pl.ds(pl.multiple_of(other * HALF, HALF), HALF)
    c_tok = fetch(tok, X.at[0])
    c_gain = fetch(gain, GN)
    group = [(wk, K0, 256), (wf, F0, 256), (wv, V0, 512), (wc, C0, 512), (wh, H0, 512),
             (wb, B0, 512), (wg, G0, 512), (wq, Q0, 256)]
    c_own = [fetch(w.at[own], W.at[0, :, pl.ds(o, n)]) for w, o, n in group[:3]]
    c_bias = fetch(bias, BI)
    c_extra = fetch(extra, EX)
    c_own += [fetch(w.at[own], W.at[0, :, pl.ds(o, n)]) for w, o, n in group[3:]]
    c_oth = [fetch(w.at[oth], W.at[1, :, pl.ds(o, n)]) for w, o, n in group]
    c_init = fetch(init, ST)
    c_taps = fetch(taps, TP_)
    c_hg = fetch(hgain, HG)
    c_wco = fetch(wco, WO.at[0])
    c_wao = fetch(wao, WO.at[1])

    c_tok.wait()
    c_gain.wait()

    def prepare(slot, which):
        xs = X[slot].astype(F32)
        g = GN[:, pl.ds(pl.multiple_of(which * HALF, HALF), HALF)]
        XG[slot] = (xs * g).astype(BF16)
        return jnp.sum(xs * xs, axis=1, keepdims=True)

    ss = prepare(0, tp)
    SS[...] = jnp.broadcast_to(ss, (ROWS, 128))

    def own_half(o, n):
        PJ[:, o:o + n] = dot(XG[0], W[0, :, o:o + n])

    c_own[0].wait()
    c_own[1].wait()
    own_half(K0, 512)
    c_own[2].wait()
    own_half(V0, 512)

    pl.semaphore_wait(bar, 1 + (PLANE - 1) + (PLANES - 1) + 2)
    tok_copy = pltpu.make_async_remote_copy(
        X.at[0], X.at[1], tok_s, tok_r, device_id=(sp, other), device_id_type=MESH
    )
    tok_copy.start()

    for i, o in ((3, C0), (4, H0), (5, B0), (6, G0)):
        c_own[i].wait()
        own_half(o, 512)
    c_own[7].wait()
    own_half(Q0, 256)

    tok_copy.wait_recv()
    ss1 = prepare(1, other)
    ss_all = SS[...] + jnp.broadcast_to(ss1, (ROWS, 128))
    RS[...] = lax.rsqrt(ss_all * (1.0 / (2 * HALF)) + NORM_EPS)

    def full(o, n):
        acc = PJ[:, o:o + n] + dot(XG[1], W[1, :, o:o + n])
        r = RS[...]
        return acc * jnp.concatenate([r] * (n // 128), axis=1)

    c_oth[0].wait()
    c_oth[1].wait()
    PJ[:, K0:K0 + 512] = full(K0, 512)
    c_oth[2].wait()
    PJ[:, V0:V0 + 512] = full(V0, 512)

    c_bias.wait()
    c_extra.wait()
    ex = (iota((8, 256), 1) // 32 == iota((8, 256), 0)).astype(BF16)
    e1, e2, e3 = split3(EX[...])
    spread = dot(e1, ex) + dot(e2, ex) + dot(e3, ex)
    pre = PJ[:, F0:F0 + 256] + BI[...]
    ls = (jnp.minimum(pre, 0.0) - jnp.log1p(jnp.exp(-jnp.abs(pre)))) * (1.0 / 16.0)
    ld_hi, ld_lo = split2(ls + spread)
    low = (iota((BLK, 2 * BLK), 0) >= iota((BLK, 2 * BLK), 1) % BLK).astype(BF16)
    tot = []
    kd = []
    for n in range(NBLK):
        rows = slice(n * BLK, (n + 1) * BLK)
        c = dot(low, jnp.concatenate([ld_hi[rows], ld_lo[rows]], axis=0))
        CUM[rows] = c
        t = c[BLK - 1:BLK]
        tot.append(t)
        kd.append(PJ[rows, K0:K0 + 256] * jnp.exp(t - c))
    later = [tot[1] + tot[2], tot[2], None]
    kf = [kd[n] * jnp.exp(later[n]) if later[n] is not None else kd[n] for n in range(NBLK)]
    kft = jnp.concatenate([x.T for x in kf], axis=1).astype(BF16)
    vb = PJ[:, V0:V0 + 512].astype(BF16)
    lane_lo = iota((32, 128), 1) < 64

    tot_all = tot[0] + tot[1] + tot[2]
    rr, jj = iota((128, 256), 0), iota((128, 256), 1)
    pick = jnp.logical_and(jj // 64 == rr // 32, jj % 32 == rr % 32)
    d1, d2, d3 = split3(jnp.where(pick, jnp.broadcast_to(tot_all, (128, 256)), 0.0))
    par = ((iota((256, 128), 0) // 32) % 2 == iota((256, 128), 1) // 64).astype(BF16)
    dec = jnp.exp(dot(d1, par) + dot(d2, par) + dot(d3, par))
    for g in range(2):
        u = dot(kft[g * 128:(g + 1) * 128], vb[:, g * 256:(g + 1) * 256])
        for half in range(2):
            a = u[half * 64:half * 64 + 32, half * 128:half * 128 + 128]
            b = u[half * 64 + 32:half * 64 + 64, half * 128:half * 128 + 128]
            comp = jnp.where(lane_lo, a, b)
            for i in range(4):
                s = (g * 2 + half) * 4 + i
                P1S[s, 0:8] = comp[i * 8:i * 8 + 8]
    for s in range(PLANE):
        P1S[s, 8:16] = dec[s * 8:s * 8 + 8]

    p1 = []
    for o in range(1, PLANE):
        q = (p + o) % PLANE
        c = pltpu.make_async_remote_copy(
            P1S.at[q], P1R.at[p], p1_s.at[o], p1_r.at[p], device_id=(base + q, tp), device_id_type=MESH
        )
        c.start()
        p1.append(c)
    P1R[p] = P1S[p]

    c_oth[3].wait()
    c_oth[4].wait()
    PR[8:8 + ROWS] = full(C0, 512)
    PR[8:8 + ROWS] = PR[8:8 + ROWS] * full(H0, 512)
    cv = pltpu.make_async_remote_copy(
        PR.at[pl.ds(ROWS, 8)], PR.at[pl.ds(0, 8)], cv_s, cv_r,
        device_id=((sp + 1) % nsp, tp), device_id_type=MESH,
    )
    cv.start()
    c_oth[5].wait()
    PJ[:, B0:B0 + 512] = full(B0, 512)

    for o in range(1, PLANE):
        q = (p + o) % PLANE
        pltpu.make_async_remote_copy(
            P1S.at[q], P1R.at[q], p1_s.at[o], p1_r.at[q], device_id=(base + q, tp), device_id_type=MESH
        ).wait_recv()
    eu = jnp.zeros((8, 128), F32)
    ed = jnp.ones((8, 128), F32)
    for q in range(PLANE):
        EU[q] = eu
        ED[q] = ed
        d = P1R[q, 8:16]
        eu = d * eu + P1R[q, 0:8]
        ed = d * ed
    ZS[0:8] = eu
    ZS[8:16] = ed
    zc = []
    for o in range(1, PLANES):
        t = (z + o) % PLANES
        c = pltpu.make_async_remote_copy(
            ZS, ZR.at[z], z_s.at[o], z_r.at[z], device_id=(t * PLANE + p, tp), device_id_type=MESH
        )
        c.start()
        zc.append(c)
    ZR[z] = ZS[...]

    c_oth[6].wait()
    c_hg.wait()
    gt = full(G0, 512)
    hg = jnp.concatenate([HG[...]] * 8, axis=1)
    PJ[:, G0:G0 + 512] = gt * jax.nn.sigmoid(gt) * hg
    c_oth[7].wait()
    PJ[:, Q0:Q0 + 256] = full(Q0, 256) * (32.0 ** -0.5)

    run = None
    for n in range(NBLK):
        rows = slice(n * BLK, (n + 1) * BLK)
        c = CUM[rows]
        t, m = c[BLK - 1:BLK], c[63:64]
        q, k = PJ[rows, Q0:Q0 + 256], PJ[rows, K0:K0 + 256]
        qi = q * jnp.exp(c)
        QI[rows] = qi.astype(BF16)
        QF[rows] = (qi if run is None else qi * jnp.exp(run)).astype(BF16)
        QG[rows] = (q * jnp.exp(c - m)).astype(BF16)
        KG[rows] = (k * jnp.exp(m - c)).astype(BF16)
        run = t if run is None else run + t
    diag = (iota((128, 256), 0) // 32 == iota((128, 256), 1) // 64)
    kd0 = PJ[0:BLK, K0:K0 + 256] * jnp.exp(CUM[BLK - 1:BLK] - CUM[0:BLK])
    kd1 = PJ[BLK:2 * BLK, K0:K0 + 256] * jnp.exp(CUM[2 * BLK - 1:2 * BLK] - CUM[BLK:2 * BLK])
    kd0t = kd0.T
    kd01t = (kd0 * jnp.exp(CUM[2 * BLK - 1:2 * BLK])).T
    kd1t = kd1.T
    e2t = jnp.concatenate([kd01t, kd1t], axis=1).astype(BF16)
    e1t = kd0t.astype(BF16)
    causal = iota((BLK, 512), 0) >= iota((BLK, 512), 1) % BLK
    for g in range(2):
        kc = slice(g * 128, (g + 1) * 128)
        vc = slice(V0 + g * 256, V0 + (g + 1) * 256)
        oc = slice(g * 256, (g + 1) * 256)
        EN[0] = jnp.where(diag, dot(e1t[kc], PJ[0:BLK, vc].astype(BF16)), 0.0).astype(BF16)
        EN[1] = jnp.where(diag, dot(e2t[kc], PJ[0:2 * BLK, vc].astype(BF16)), 0.0).astype(BF16)
        for n in range(NBLK):
            rows = slice(n * BLK, (n + 1) * BLK)
            kg = KG[rows, kc].astype(F32)
            vv = PJ[rows, vc]
            kl, vl = iota((BLK, 128), 1) // 32, iota((BLK, 256), 1) // 64
            km = jnp.concatenate([jnp.where(kl == a, kg, 0.0).astype(BF16) for a in range(4)], axis=0)
            vm = jnp.concatenate([jnp.where(vl == a, vv, 0.0).astype(BF16) for a in range(4)], axis=0)
            s = jnp.where(causal, dot_t(QG[rows, kc], km), 0.0).astype(BF16)
            r = dot(s, vm)
            if n > 0:
                r = r + dot(QI[rows, kc], EN[n - 1])
            RAW[rows, oc] = r

    c_init.wait()
    for pr in range(4):
        INI[pr * 32:pr * 32 + 32] = jnp.concatenate([ST[2 * pr], ST[2 * pr + 1]], axis=1)
    for o in range(1, PLANES):
        t = (z + o) % PLANES
        pltpu.make_async_remote_copy(
            ZS, ZR.at[t], z_s.at[o], z_r.at[t], device_id=(t * PLANE + p, tp), device_id_type=MESH
        ).wait_recv()
    state = INI[pl.ds(pl.multiple_of(p * 8, 8), 8)]
    for t in range(PLANES):
        new = ZR[t, 8:16] * state + ZR[t, 0:8]
        state = jnp.where(t < z, new, state)
    for q in range(PLANE):
        P3S[q] = EU[q] + ED[q] * state
    p3 = []
    for o in range(1, PLANE):
        q = (p + o) % PLANE
        c = pltpu.make_async_remote_copy(
            P3S.at[q], SIN.at[p], p3_s.at[o], p3_r.at[p], device_id=(base + q, tp), device_id_type=MESH
        )
        c.start()
        p3.append(c)
    SIN[p] = P3S[p]

    cv.wait_recv()
    c_taps.wait()
    PR[0:8] = jnp.where(sp > 0, PR[0:8], 0.0)
    tw = TP_[...].astype(F32)
    conv = tw[0:1] * PR[6:6 + ROWS] + tw[1:2] * PR[7:7 + ROWS] + tw[2:3] * PR[8:8 + ROWS]
    CO[...] = (PJ[:, B0:B0 + 512] * conv).astype(BF16)
    c_wco.wait()
    for j in range(4):
        OUT[:, j * 512:(j + 1) * 512] = dot(CO[...], WO[0, :, j * 512:(j + 1) * 512])

    for o in range(1, PLANE):
        q = (p + o) % PLANE
        pltpu.make_async_remote_copy(
            P3S.at[q], SIN.at[q], p3_s.at[o], p3_r.at[q], device_id=(base + q, tp), device_id_type=MESH
        ).wait_recv()
    ones = (iota((256, 256), 0) // 64 == iota((256, 256), 1) // 64).astype(BF16)
    zero = jnp.zeros((32, 128), F32)
    for g in range(2):
        kc = slice(g * 128, (g + 1) * 128)
        oc = slice(g * 256, (g + 1) * 256)
        parts = []
        for half in range(2):
            s0 = (g * 2 + half) * 4
            comp = jnp.concatenate([SIN[s0 + i] for i in range(4)], axis=0)
            for lo in (True, False):
                mine = jnp.where(lane_lo if lo else jnp.logical_not(lane_lo), comp, 0.0)
                parts.append(jnp.concatenate([mine, zero] if half == 0 else [zero, mine], axis=1))
        sbd = jnp.concatenate(parts, axis=0).astype(BF16)
        raw = RAW[:, oc] + dot(QF[:, kc], sbd)
        ms = dot((raw * raw).astype(BF16), ones) * (1.0 / 64.0)
        AO[:, oc] = (raw * lax.rsqrt(ms + NORM_EPS) * PJ[:, G0 + g * 256:G0 + (g + 1) * 256]).astype(BF16)

    c_wao.wait()
    his = pl.ds(pl.multiple_of(other * 192, 64), 192)
    mine = pl.ds(pl.multiple_of(tp * 192, 64), 192)
    oc_copies = []
    for j in range(4):
        cols = slice(j * 512, (j + 1) * 512)
        SB[j] = (OUT[his, cols] + dot(AO[his], WO[1, :, cols])).astype(BF16)
        c = pltpu.make_async_remote_copy(
            SB.at[j], RB.at[j], ot_s.at[j], ot_r.at[j], device_id=(sp, other), device_id_type=MESH
        )
        c.start()
        oc_copies.append(c)
    for j in range(4):
        cols = slice(j * 512, (j + 1) * 512)
        OUT[mine, cols] = OUT[mine, cols] + dot(AO[mine], WO[1, :, cols])
    fin = []
    for j in range(4):
        cols = slice(j * 512, (j + 1) * 512)
        oc_copies[j].wait_recv()
        OB[:, cols] = (OUT[mine, cols] + RB[j].astype(F32)).astype(BF16)
        c = pltpu.make_async_copy(OB.at[:, cols], out.at[:, cols], osem.at[j])
        c.start()
        fin.append(c)
    tok_copy.wait_send()
    cv.wait_send()
    for c in p1 + zc + p3 + oc_copies:
        c.wait_send()
    for c in fin:
        c.wait()


def on_device(
    tokens, input_norm_gain, outer_gate_weight, inner_gate_weight, convolution_input_weight,
    convolution_kernel_taps, query_weight_matrix, key_weight_matrix, value_weight_matrix,
    forget_gate_weight, attention_gate_weight, forget_gate_bias, extra_logarithm_decay,
    initial_head_state, head_norm_gain, convolution_output_weight, attention_output_weight,
):
    dma, reg = pltpu.SemaphoreType.DMA, pltpu.SemaphoreType.REGULAR
    v = pltpu.VMEM
    scratch = [
        v((2, ROWS, HALF), BF16),
        v((2, ROWS, HALF), BF16),
        v((2, HALF, WIDE), BF16),
        v((2, 512, 2048), BF16),
        v((ROWS, WIDE), F32),
        v((ROWS, 128), F32),
        v((ROWS, 128), F32),
        v((1, 2048), F32),
        v((1, 256), F32),
        v((ROWS, 8), F32),
        v((3, 512), BF16),
        v((1, 64), F32),
        v((8, 32, 64), F32),
        v((ROWS, 256), F32),
        v((ROWS, 256), BF16),
        v((ROWS, 256), BF16),
        v((ROWS, 256), BF16),
        v((ROWS, 256), BF16),
        v((2, 128, 256), BF16),
        v((PLANE, 16, 128), F32),
        v((PLANE, 16, 128), F32),
        v((PLANE, 8, 128), F32),
        v((PLANE, 8, 128), F32),
        v((16, 128), F32),
        v((PLANES, 16, 128), F32),
        v((PLANE, 8, 128), F32),
        v((PLANE, 8, 128), F32),
        v((128, 256), BF16),
        v((128, 128), F32),
        v((ROWS + 8, 512), F32),
        v((ROWS, 512), BF16),
        v((ROWS, 512), F32),
        v((ROWS, 512), BF16),
        v((ROWS, 2048), F32),
        v((4, 192, 512), BF16),
        v((4, 192, 512), BF16),
        v((192, 2048), BF16),
        dma((25,)), dma((4,)), dma, dma,
        dma((PLANE,)), dma((PLANE,)), dma((PLANES,)), dma((PLANES,)), dma((PLANE,)), dma((PLANE,)),
        dma, dma, dma((4,)), dma((4,)),
    ]
    return pl.pallas_call(
        kernel,
        out_shape=jax.ShapeDtypeStruct((192, 2048), BF16),
        in_specs=[pl.BlockSpec(memory_space=pl.ANY)] * 17,
        out_specs=pl.BlockSpec(memory_space=pl.ANY),
        scratch_shapes=scratch,
        compiler_params=pltpu.CompilerParams(
            collective_id=0, has_side_effects=True, vmem_limit_bytes=60 * 1024 * 1024
        ),
        name="layer",
    )(
        tokens, input_norm_gain.reshape(1, -1), outer_gate_weight, inner_gate_weight,
        convolution_input_weight, convolution_kernel_taps, query_weight_matrix, key_weight_matrix,
        value_weight_matrix, forget_gate_weight, attention_gate_weight, forget_gate_bias.reshape(1, -1),
        extra_logarithm_decay, initial_head_state, head_norm_gain.reshape(1, -1),
        convolution_output_weight, attention_output_weight,
    )


def solution(mesh):
    return jax.shard_map(
        on_device,
        mesh=mesh,
        in_specs=(
            P("sp", "tp"), P(), P(None, "tp"), P(None, "tp"), P(None, "tp"), P(None, "tp"),
            P(None, "tp"), P(None, "tp"), P(None, "tp"), P(None, "tp"), P(None, "tp"),
            P("tp"), P("sp", "tp"), P("tp", None, None), P(), P("tp", None), P("tp", None),
        ),
        out_specs=P(("sp", "tp"), None),
        check_vma=False,
    )
```

time: 189 us -> 39.6 us (0.21)
  blocking collectives: 71.1 us -> 0 us
  local copies, waits for them, and re-layouts: 52.3 us -> 3.6 us
  matrix products: 36.5 us -> 0 us
  Pallas kernels: 0 us -> 35.8 us
  other arithmetic: 25.1 us -> 0 us
  starting transfers between devices: 1.97 us -> 0 us
    all_gather x3 -> x0, blocking collectives: 44 us -> none  [collected_together(): both, at, found = (lax.all_gather(jnp.concatenate(lines), axis), 0, {})]
    dot_general x12 -> x0, matrix products: 36.5 us -> none  [the longest x6 11.4 us: on_device(): jnp.dot(normed, weight, preferred_element_type=jnp.float32)]
    pallas_call x0 -> x1, Pallas kernels: none -> 35.8 us  [on_device(): pl.pallas_call(kernel, out_shape=jax.ShapeDtypeStruct((192, 2048), BF16),...]
    all_to_all x2 -> x0, blocking collectives: 27.1 us -> none  [the longest x1 19.3 us: sent_and_summed(): lax.all_to_all(parts, axis, split_axis=0, concat_axis=0, tiled=True)]
    unnamed x126 -> x2, local copies, waits for them, and re-layouts: 14.9 us -> 3.6 us
    reshape x5 -> x0, local copies, waits for them, and re-layouts: 9.65 us -> none  [the longest x1 2.73 us: on_device(): (query.astype(jnp.float32) * key_channel_count ** (-0.5)).reshape(n_block...]
    mul x27 -> x0, local copies, waits for them, and re-layouts: 8.7 us -> none  [the longest x16 5.46 us: chain_join(): return (earlier[0] * later[0], later[0][..., None] * earlier[1] + later[1])]
    slice x15 -> x0, local copies, waits for them, and re-layouts: 8.68 us -> none  [the longest x14 8.09 us: entering_2(): so_far = combine(so_far, jax.tree.map(lambda part: part[k], pieces))]
  transfers between devices with their start and end apart: 1 -> 0, of which waited for: 0 -> 0; matrix products, arithmetic and copies ran while one was open for 47% -> 0% of each run, Pallas kernels for 0% -> 0%
where the time goes in v1:
time: 39.6 us; the launch traced here: 39.4 us
  Pallas kernels  35.8 us (90%)
  local copies, waits for them, and re-layouts  3.6 us (9%)
    pallas_call x1, Pallas kernels, on_device(): pl.pallas_call(kernel, out_shape=jax.ShapeDtypeStruct((192, 2048), BF16),...  35.8 us
    unnamed x2, local copies, waits for them, and re-layouts  3.6 us

profile of v1, /device:TPU:1, one launch (start us, length us, event | category | flops | bytes accessed | tf_op | source)
XLA Modules:
  0.0 39.4 jit_solution(7468118697495936522)
XLA Ops:
  0.0 1.5 %copy.18.extra = f32[384,8]{1,0:T(8,128)} copy(f32[384,8]{0,1:T(8,128)} %param.29) | data formatting | bytes 24576 | tf_op args[12]
  1.5 35.8 %layer.1 = bf16[192,2048]{1,0:T(8,128)(2,1)} custom-call(bf16[384,1024]{1,0:T(8,128)(2,1)} %tok.1, f32[1,2048]{1,0:T(1,128)} %bitcast.3, bf16[2048,512]{1,0:T(8,128)(2,1)} %wb.1, bf16[2048,512]{1,0:T(8,128)(2,1)} %wc.1, bf16[2048,512]{1,0:T(8,128)(2,1)} %wh.1, bf16[3,512]{1,0:T(4,128)(2,1)} %taps.1, bf16[2048,256]{1,0:T(8,128)(2,1)} %wq.1, ...), custom_call_target="tpu_custom_call" | custom-call | tf_op jit(solution)/shard_map/layer/pallas_call | solution.py:425
  37.3 2.1 %copy.20 = bf16[192,2048]{1,0:T(8,128)(2,1)} copy(bf16[192,2048]{1,0:T(8,128)(2,1)} %layer.1) | data formatting | bytes 1572864
